TPU v7x, 32 devices: a whole 2x2x4 slice. The times are simulated.
32 devices in a mesh: sp: 8 (over z, y), tp: 4 (over x, core).
Axes of the slice: x: 2, y: 2, z: 4, core: 2. Of those that a mesh axis runs over, the one named last changes fastest.
Arguments:
- stream: bfloat16 [2048, 2048], P('sp'), may hold values from -3 to 3
- first_group_queries: bfloat16 [2048, 512], P('sp', 'tp'), may hold values from -6 to 6
- first_group_keys: bfloat16 [2048, 512], P('sp', 'tp'), may hold values from -6 to 6
- first_group_values: bfloat16 [2048, 1024], P('sp', 'tp'), may hold values from -5.5 to 5.5
- first_gate_logits: bfloat16 [2048, 1024], P('sp', 'tp'), may hold values from -6 to 6
- first_decay_logits: bfloat16 [2048, 512], P('sp', 'tp'), may hold values from -4.75 to 14.5
- second_group_queries: bfloat16 [2048, 1024], P('sp', 'tp'), may hold values from -6 to 6
- second_group_keys: bfloat16 [2048, 1024], P('sp', 'tp'), may hold values from -6 to 6
- second_group_values: bfloat16 [2048, 1024], P('sp', 'tp'), may hold values from -5.5 to 5.5
- second_gate_logits: bfloat16 [2048, 1024], P('sp', 'tp'), may hold values from -6 to 6
- second_decay_logits: bfloat16 [2048, 1024], P('sp', 'tp'), may hold values from -4.75 to 14.5
- position_log_decay: float32 [2048], P('sp'), may hold values from -0.6932 to 0, as said below
- per_head_norm_gain: float32 [128], replicated, may hold values from 0.1 to 1.9
- first_output_weight: bfloat16 [1024, 2048], P('tp'), may hold values from -0.125 to 0.125
- second_output_weight: bfloat16 [1024, 2048], P('tp'), may hold values from -0.125 to 0.125
- feedforward_norm_gain: float32 [2048], replicated, may hold values from 0.1 to 1.9
- gate_weight: bfloat16 [2048, 5632], P('sp', 'tp'), may hold values from -0.125 to 0.125
- up_weight: bfloat16 [2048, 5632], P('sp', 'tp'), may hold values from -0.125 to 0.125
- down_weight: bfloat16 [5632, 2048], P('tp', 'sp'), may hold values from -0.078125 to 0.078125
Outputs:
- refined: bfloat16 [2048, 2048], P(('sp', 'tp'))
Inputs may be any that keep to these rules, and one draw needn't show every extreme that they name: `position_log_decay`: most positions carry 0.
All inputs are finite; a program needn't handle non-finite values.
Results may differ from a plain program's by a relative error of at most 0.018.
Values may be sent and summed in bfloat16 or wider, within the bound.
A program may use at most 64 MiB of HBM per device.

v0:
```python
import jax
import jax.numpy as jnp
from jax import lax
from jax.sharding import PartitionSpec as P

KEY_SIZE_FIRST = 64
KEY_SIZE_SECOND = 128
DV = 128
BLK = 64
decay_softness = 16.0
norm_eps = 1e-06
highest = lax.Precision.HIGHEST


def channel_log_decays(decay_logits, position_log_decay, key_channels):
    channel_log_decay = (
        jax.nn.log_sigmoid(decay_logits.astype(jnp.float32)) / decay_softness
        + position_log_decay[:, None]
    )
    return channel_log_decay.reshape(decay_logits.shape[0], -1, key_channels)


def one_way(query_matrix, key_matrix, value_matrix, channel_log_decay, start_state):
    length, heads, key_channels = query_matrix.shape
    value_width = value_matrix.shape[-1]
    block_count = length // BLK

    def blocks(member):
        return member.reshape(block_count, BLK, heads, member.shape[-1]).transpose(0, 2, 1, 3)

    query_blocks = blocks(query_matrix)
    key_blocks = blocks(key_matrix)
    value_blocks = blocks(value_matrix)
    running = jnp.cumsum(blocks(channel_log_decay), axis=2)
    block_last = running[:, :, -1:, :]
    query_in = query_blocks * jnp.exp(running)
    key_in = key_blocks * jnp.exp(-running)
    key_end = key_blocks * jnp.exp(block_last - running)
    places = jnp.arange(BLK, dtype=jnp.int32)
    lower = places[:, None] >= places[None, :]
    scores = jnp.where(
        lower, jnp.einsum("nhid,nhjd->nhij", query_in, key_in, precision=highest), 0.0
    )
    local_out = jnp.einsum("nhij,nhjv->nhiv", scores, value_blocks, precision=highest)

    def advance(states, inputs):
        query_part, key_part, value_part, last_part = inputs
        emitted = jnp.einsum("hid,hdv->hiv", query_part, states, precision=highest)
        states = states * jnp.exp(last_part)[:, 0, :, None] + jnp.einsum(
            "hjd,hjv->hdv", key_part, value_part, precision=highest
        )
        return (states, emitted)

    _, carried = lax.scan(advance, start_state, (query_in, key_end, value_blocks, block_last))
    return (local_out + carried).transpose(0, 2, 1, 3).reshape(length, heads, value_width)


def prepare_inputs(
    query_matrix, key_matrix, value_matrix, decay_logits, position_log_decay, key_channels
):
    length = query_matrix.shape[0]
    channel_log_decay = channel_log_decays(decay_logits, position_log_decay, key_channels)
    query_f = query_matrix.astype(jnp.float32).reshape(length, -1, key_channels)
    key_f = key_matrix.astype(jnp.float32).reshape(length, -1, key_channels)
    value_f = value_matrix.astype(jnp.float32).reshape(length, -1, DV)
    return (query_f, key_f, value_f, channel_log_decay)


def flipped(members):
    return tuple((jnp.flip(member, axis=0) for member in members))


def end_state(members):
    key_f, value_f, channel_log_decay = (members[1], members[2], members[3])
    totals = jnp.sum(channel_log_decay, axis=0)
    running = jnp.cumsum(channel_log_decay, axis=0)
    weighted = key_f * jnp.exp(totals[None] - running)
    states = jnp.einsum("thd,thv->hdv", weighted, value_f, precision=highest)
    return (totals, states)


def finish(forward, backward, gate_values, per_head_norm_gain):
    both = forward + backward
    scale = lax.rsqrt(jnp.mean(both * both, axis=-1, keepdims=True) + norm_eps)
    gated = (
        both
        * scale
        * per_head_norm_gain
        * jax.nn.silu(gate_values.astype(jnp.float32).reshape(both.shape))
    )
    return gated.reshape(both.shape[0], -1).astype(jnp.bfloat16)


def rms_rows(rows, feedforward_norm_gain):
    scale = lax.rsqrt(jnp.mean(rows * rows, axis=-1, keepdims=True) + norm_eps)
    return (rows * scale * feedforward_norm_gain).astype(jnp.bfloat16)


def per_device(
    stream,
    first_group_queries,
    first_group_keys,
    first_group_values,
    first_gate_logits,
    first_decay_logits,
    second_group_queries,
    second_group_keys,
    second_group_values,
    second_gate_logits,
    second_decay_logits,
    position_log_decay,
    per_head_norm_gain,
    first_output_weight,
    second_output_weight,
    feedforward_norm_gain,
    gate_weight,
    up_weight,
    down_weight,
):
    tok_rows = stream.shape[0]
    first_group = prepare_inputs(
        first_group_queries,
        first_group_keys,
        first_group_values,
        first_decay_logits,
        position_log_decay,
        KEY_SIZE_FIRST,
    )
    second_group = prepare_inputs(
        second_group_queries,
        second_group_keys,
        second_group_values,
        second_decay_logits,
        position_log_decay,
        KEY_SIZE_SECOND,
    )
    first_back = flipped(first_group)
    second_back = flipped(second_group)
    ahead_first = end_state(first_group)
    ahead_second = end_state(second_group)
    behind_first = end_state(first_back)
    behind_second = end_state(second_back)
    all_first, all_second = (
        lax.all_gather(ahead_first[0][None], "sp", axis=0, tiled=True),
        lax.all_gather(ahead_second[0][None], "sp", axis=0, tiled=True),
    )
    own_place = lax.axis_index("sp")

    def weights_for(all_logs, count):
        running = jnp.cumsum(all_logs, axis=0)
        own_end = running[own_place]
        own_before = own_end - all_logs[own_place]
        their_before = running - all_logs
        ranks = jnp.arange(count, dtype=jnp.int32)
        lower = (ranks < own_place)[:, None, None]
        higher = (ranks > own_place)[:, None, None]
        ahead = jnp.exp(jnp.where(lower, own_before - running, -jnp.inf))
        behind = jnp.exp(jnp.where(higher, their_before - own_end, -jnp.inf))
        return (ahead, behind)

    empty = (
        jnp.zeros_like(ahead_first[1]),
        jnp.zeros_like(ahead_first[1]),
        jnp.zeros_like(ahead_second[1]),
        jnp.zeros_like(ahead_second[1]),
    )
    pieces = (
        lax.all_gather(ahead_first[1][None].astype(jnp.bfloat16), "sp", axis=0, tiled=True).astype(
            jnp.float32
        ),
        lax.all_gather(behind_first[1][None].astype(jnp.bfloat16), "sp", axis=0, tiled=True).astype(
            jnp.float32
        ),
        lax.all_gather(ahead_second[1][None].astype(jnp.bfloat16), "sp", axis=0, tiled=True).astype(
            jnp.float32
        ),
        lax.all_gather(
            behind_second[1][None].astype(jnp.bfloat16), "sp", axis=0, tiled=True
        ).astype(jnp.float32),
    )
    count = pieces[0].shape[0]
    ahead_a, behind_a = weights_for(all_first, count)
    ahead_b, behind_b = weights_for(all_second, count)
    forward_first = one_way(
        first_group[0],
        first_group[1],
        first_group[2],
        first_group[3],
        empty[0] + jnp.einsum("nhd,nhdv->hdv", ahead_a, pieces[0], precision=highest),
    )
    backward_first = jnp.flip(
        one_way(
            first_back[0],
            first_back[1],
            first_back[2],
            first_back[3],
            empty[1] + jnp.einsum("nhd,nhdv->hdv", behind_a, pieces[1], precision=highest),
        ),
        0,
    )
    forward_second = one_way(
        second_group[0],
        second_group[1],
        second_group[2],
        second_group[3],
        empty[2] + jnp.einsum("nhd,nhdv->hdv", ahead_b, pieces[2], precision=highest),
    )
    backward_second = jnp.flip(
        one_way(
            second_back[0],
            second_back[1],
            second_back[2],
            second_back[3],
            empty[3] + jnp.einsum("nhd,nhdv->hdv", behind_b, pieces[3], precision=highest),
        ),
        0,
    )
    first_group_output = finish(
        forward_first, backward_first, first_gate_logits, per_head_norm_gain
    )
    second_group_output = finish(
        forward_second, backward_second, second_gate_logits, per_head_norm_gain
    )
    part_rows = tok_rows // lax.axis_size("tp")
    row_start = lax.axis_index("tp") * part_rows
    summed = lax.psum(
        (
            jnp.dot(first_group_output, first_output_weight, preferred_element_type=jnp.float32)
            + jnp.dot(second_group_output, second_output_weight, preferred_element_type=jnp.float32)
        ).astype(jnp.bfloat16),
        "tp",
    ).astype(jnp.float32)
    residual = stream.astype(jnp.float32) + summed
    normed_all = rms_rows(residual, feedforward_norm_gain)
    own_residual = lax.dynamic_slice_in_dim(residual, row_start, part_rows, 0)
    pieces = (
        lax.all_gather(gate_weight, "sp", axis=0, tiled=True),
        lax.all_gather(up_weight, "sp", axis=0, tiled=True),
    )
    gate_sum = jnp.dot(normed_all, pieces[0], preferred_element_type=jnp.float32)
    up_sum = jnp.dot(normed_all, pieces[1], preferred_element_type=jnp.float32)
    hidden = (jax.nn.silu(gate_sum) * up_sum).astype(jnp.bfloat16)
    down_whole = lax.all_gather(down_weight, "sp", axis=1, tiled=True)
    down_sum = lax.psum_scatter(
        jnp.dot(hidden, down_whole, preferred_element_type=jnp.float32).astype(jnp.bfloat16),
        "tp",
        scatter_dimension=0,
        tiled=True,
    ).astype(jnp.float32)
    return (own_residual + 0.5 * down_sum).astype(jnp.bfloat16)


def solution(mesh):
    in_specs = (
        P("sp", None),
        P("sp", "tp"),
        P("sp", "tp"),
        P("sp", "tp"),
        P("sp", "tp"),
        P("sp", "tp"),
        P("sp", "tp"),
        P("sp", "tp"),
        P("sp", "tp"),
        P("sp", "tp"),
        P("sp", "tp"),
        P("sp"),
        P(),
        P("tp", None),
        P("tp", None),
        P(),
        P("sp", "tp"),
        P("sp", "tp"),
        P("tp", "sp"),
    )
    out_specs = P(("sp", "tp"), None)
    return jax.shard_map(
        per_device, mesh=mesh, in_specs=in_specs, out_specs=out_specs, check_vma=False
    )
```

profile of v0, /device:TPU:0, one launch (start us, length us, event | category | flops | bytes accessed | tf_op | source)
XLA Modules:
  0.0 579.6 jit_solution(15194093987630395146)
XLA Ops:
  7.4 1.0 copy.247
  8.4 0.9 fusion.78
  10.8 0.9 copy.244
  12.8 0.9 reshape.254
  16.2 1.0 reshape.255
  17.4 1.1 reshape.256
  20.7 22.3 %all_gather.27 = f32[8,2,64]{2,1,0:T(2,128)S(1)} all-gather(f32[1,2,64]{2,1,0:T(2,128)S(1)} %broadcast_in_dim.108), channel_id=1, replica_groups=mesh['sp'=8,'tp'=4] {'sp'}, dimensions={0}, use_global_device_ids=true | all-gather | bytes 4608 | tf_op jit(solution)/shard_map/all_gather | solution.py:144
  43.9 1.2 reduce-window.30
  46.7 32.8 %all-gather.1 = bf16[16,64,128]{2,1,0:T(8,128)(2,1)} all-gather(bf16[2,64,128]{2,1,0:T(8,128)(2,1)S(1)} %convolution_convert_fusion.4), channel_id=3, replica_groups=mesh['sp'=8,'tp'=4] {'sp'}, dimensions={0}, use_global_device_ids=true | all-gather | bytes 294912 | tf_op jit(solution)/shard_map/all_gather | solution.py:171
  80.6 1.6 fusion.71
  83.0 4.6 while.49
  88.2 1.4 fusion.44
  90.5 1.2 reduce-window.26
  92.3 32.8 %all-gather = bf16[16,64,128]{2,1,0:T(8,128)(2,1)} all-gather(bf16[2,64,128]{2,1,0:T(8,128)(2,1)S(1)} %convolution_convert_fusion.3), channel_id=2, replica_groups=mesh['sp'=8,'tp'=4] {'sp'}, dimensions={0}, use_global_device_ids=true | all-gather | bytes 294912 | tf_op jit(solution)/shard_map/all_gather | solution.py:168
  126.8 1.6 fusion.73
  128.4 2.3 while.48
  132.2 16.3 %all_gather.30 = f32[8,2,128]{2,1,0:T(2,128)S(1)} all-gather(f32[1,2,128]{2,1,0:T(2,128)S(1)} %bitcast.424), channel_id=1, replica_groups=mesh['sp'=8,'tp'=4] {'sp'}, dimensions={0}, use_global_device_ids=true | all-gather | bytes 9216 | tf_op jit(solution)/shard_map/all_gather | solution.py:145
  153.3 2.0 rev.40
  155.5 1.4 convolution_convert_fusion.1
  156.9 33.5 %all-gather.3 = bf16[16,128,128]{2,1,0:T(8,128)(2,1)} all-gather(bf16[2,128,128]{2,1,0:T(8,128)(2,1)S(1)} %convolution_convert_fusion.1), channel_id=5, replica_groups=mesh['sp'=8,'tp'=4] {'sp'}, dimensions={0}, use_global_device_ids=true | all-gather | bytes 589824 | tf_op jit(solution)/shard_map/all_gather | solution.py:177
  190.5 1.0 copy.305
  191.7 1.6 rev.37
  193.3 1.1 copy.302
  194.3 1.3 convolution_select_fusion
  196.5 1.2 fusion.46
  198.4 8.6 %while.51 = (s32[]{:T(128)}, f32[2,128,128]{2,1,0:T(8,128)S(1)}, f32[4,2,64,128]{3,2,1,0:T(8,128)}, f32[4,2,1,128]{3,1,2,0:T(2,128)S(1)}, f32[4,2,64,128]{3,2,1,...) while((s32[]{:T(128)}, f32[2,128,128]{2,1,0:T(8,128)S(1)}, ...), condition=%wide.region_26.27_spmd, body=%wide.region_25.26_spmd.sunk | while | flops 50397184 | bytes 660569 | solution.py:54
  199.2 1.2 convolution_add_fusion.16
  201.4 1.2 convolution_add_fusion.16
  203.5 1.2 convolution_add_fusion.16
  205.7 1.2 convolution_add_fusion.16
  206.9 1.3 fusion.42
  210.5 1.1 copy.295
  212.0 33.2 %all-gather.2 = bf16[16,128,128]{2,1,0:T(8,128)(2,1)} all-gather(bf16[2,128,128]{2,1,0:T(8,128)(2,1)S(1)} %convolution_convert_fusion.2), channel_id=4, replica_groups=mesh['sp'=8,'tp'=4] {'sp'}, dimensions={0}, use_global_device_ids=true | all-gather | bytes 589824 | tf_op jit(solution)/shard_map/all_gather | solution.py:174
  245.2 1.1 reshape_reshape.34
  247.7 1.1 reshape_reshape.37
  248.7 2.2 fusion.48
  251.0 2.9 while.50
  254.4 1.0 copy.278
  257.2 1.5 fusion.41
  260.7 33.2 %all-reduce.2.cloned.1.call-done = bf16[256,2048]{1,0:T(8,128)(2,1)} async-done(((bf16[256,2048]{1,0:T(8,128)(2,1)}), bf16[256,2048]{1,0:T(8,128)(2,1)}) %all-reduce.2.cloned.1.call-update) | async-done | bytes 1048592 | tf_op jit(solution)/shard_map/psum | solution.py:226
  293.9 2.0 convert_add_fusion
  295.9 56.1 %all-gather.8.cloned.1.call-done = bf16[2048,1408]{1,0:T(8,128)(2,1)} async-done(((bf16[256,1408]{1,0:T(8,128)(2,1)}), bf16[2048,1408]{1,0:T(8,128)(2,1)}) %all-gather.8.cloned.1.call-update) | async-done | bytes 5767184 | tf_op jit(solution)/shard_map/all_gather | solution.py:237
  352.0 6.3 %fusion.112 = f32[256,1408]{1,0:T(8,128)} fusion(bf16[2048,1408]{1,0:T(8,128)(2,1)} %all-gather.8.cloned.1.call-done, f32[2048]{0:T(1024)S(1)} %copy-done.33, f32[256]{0:T(256)S(1)} %add_rsqrt_fusion.2, bf16[256,2048]{1,0:T(8,128)(2,1)} %all-reduce.2.cloned.1.call-done, bf16[256,2048]{1,0:T(8,128)(2,1)} %param.27), kind=kOutput, calls=%fused_computation.189 | convolution fusion | flops 1479540736 | bytes 9315328 | tf_op jit(solution)/shard_map/dot_general | solution.py:240
  358.3 86.1 %all-gather.10.cloned.1.call-done = bf16[2048,1408]{1,0:T(8,128)(2,1)} async-done(((bf16[256,1408]{1,0:T(8,128)(2,1)}), bf16[2048,1408]{1,0:T(8,128)(2,1)}) %all-gather.10.cloned.1.call-update) | async-done | bytes 5767184 | tf_op jit(solution)/shard_map/all_gather | solution.py:238
  444.4 93.0 %all-gather.12.cloned.1.call-done = bf16[1408,2048]{1,0:T(8,128)(2,1)} async-done(((bf16[1408,256]{1,0:T(8,128)(2,1)}), bf16[1408,2048]{1,0:T(8,128)(2,1)}) %all-gather.12.cloned.1.call-update) | async-done | bytes 5767184 | tf_op jit(solution)/shard_map/all_gather | solution.py:243
  537.3 9.9 %convolution_convert_fusion = bf16[256,2048]{1,0:T(8,128)(2,1)} fusion(bf16[1408,2048]{1,0:T(8,128)(2,1)} %all-gather.12.cloned.1.call-done, bf16[2048,1408]{1,0:T(8,128)(2,1)} %all-gather.10.cloned.1.call-done, f32[256,1408]{1,0:T(8,128)} %fusion.112, f32[2048]{0:T(1024)S(1)} %copy-done.33, f32[256]{0:T(256)S(1)} %add_rsqrt_fusion.2, ...), kind=kOutput, calls=%fused_computation.60 | convolution fusion | flops 2958622720 | bytes 16131072 | tf_op jit(solution)/shard_map/dot_general | solution.py:245
  547.2 23.1 %reduce-scatter.2.cloned.1.call-done = bf16[64,2048]{1,0:T(8,128)(2,1)} async-done(((bf16[256,2048]{1,0:T(8,128)(2,1)}), bf16[64,2048]{1,0:T(8,128)(2,1)}) %reduce-scatter.2.cloned.1.call-update) | async-done | bytes 262160 | tf_op jit(solution)/shard_map/reduce_scatter | solution.py:244
  570.3 1.7 add_convert_fusion
  (260 shorter events, 44.1 us)
Async XLA Ops:
  7.4 248.9 %copy-start = (bf16[256,2048]{1,0:T(8,128)(2,1)S(1)}, bf16[256,2048]{1,0:T(8,128)(2,1)}, u32[]{:S(2)}) copy-start(bf16[256,2048]{1,0:T(8,128)(2,1)} %param.40) | copy-start | bytes 3145732
  7.4 5.3 copy-start.23
  7.4 6.3 %copy-start.3 = (bf16[256,256]{1,0:T(8,128)(2,1)S(1)}, bf16[256,256]{1,0:T(8,128)(2,1)}, u32[]{:S(2)}) copy-start(bf16[256,256]{1,0:T(8,128)(2,1)} %param.30) | copy-start | bytes 393220
  7.4 286.5 %all-reduce.2.cloned.1.call-start = ((), (), s32[]{:S(2)}) async-start(), calls=%async_computation.1 | async-start | bytes 2097152 | tf_op jit(solution)/shard_map/psum | solution.py:226
  8.4 6.9 %copy-start.18 = (bf16[256,256]{1,0:T(8,128)(2,1)S(1)}, bf16[256,256]{1,0:T(8,128)(2,1)}, u32[]{:S(2)}) copy-start(bf16[256,256]{1,0:T(8,128)(2,1)} %param.33) | copy-start | bytes 393220
  9.7 33.3 %copy-start.28 = (pred[8]{0:T(512)(128)(4,1)}, pred[8]{0:T(512)(128)(4,1)S(1)}, u32[]{:S(2)}) copy-start(pred[8]{0:T(512)(128)(4,1)S(1)} %get-tuple-element.377) | copy-start | bytes 28
  9.7 33.3 %copy-start.30 = (pred[8]{0:T(512)(128)(4,1)}, pred[8]{0:T(512)(128)(4,1)S(1)}, u32[]{:S(2)}) copy-start(pred[8]{0:T(512)(128)(4,1)S(1)} %get-tuple-element.378) | copy-start | bytes 28
  9.9 7.3 %copy-start.19 = (bf16[256,256]{1,0:T(8,128)(2,1)S(1)}, bf16[256,256]{1,0:T(8,128)(2,1)}, u32[]{:S(2)}) copy-start(bf16[256,256]{1,0:T(8,128)(2,1)} %param.34) | copy-start | bytes 393220
  12.8 32.6 %copy-start.4 = (f32[256,128]{0,1:T(8,128)}, f32[256,128]{0,1:T(8,128)S(1)}, u32[]{:S(2)}) copy-start(f32[256,128]{0,1:T(8,128)S(1)} %convert_element_type.93) | copy-start | bytes 393220
  12.8 5.6 copy-start.6
  87.6 2.2 copy-start.25
  87.6 4.4 copy-start.5
  88.2 37.0 %copy-start.12 = (f32[4,64,2,64]{1,0,3,2:T(4,128)S(1)}, f32[4,64,2,64]{1,0,3,2:T(4,128)}, u32[]{:S(2)}) copy-start(f32[4,64,2,64]{1,0,3,2:T(4,128)} %reshape_reshape.29) | copy-start | bytes 393220
  89.6 36.0 %copy-start.8 = (f32[4,64,2,64]{1,0,3,2:T(4,128)S(1)}, f32[4,64,2,64]{1,0,3,2:T(4,128)}, u32[]{:S(2)}) copy-start(f32[4,64,2,64]{1,0,3,2:T(4,128)} %reshape.253) | copy-start | bytes 393220
  89.6 36.1 %copy-start.9 = (f32[4,64,2,64]{1,0,3,2:T(4,128)S(1)}, f32[4,64,2,64]{1,0,3,2:T(4,128)}, u32[]{:S(2)}) copy-start(f32[4,64,2,64]{1,0,3,2:T(4,128)} %reshape.254) | copy-start | bytes 393220
  125.3 1.3 copy-start.11
  126.6 4.1 copy-start.16
  128.4 3.4 copy-start.20
  128.4 3.5 copy-start.27
  130.7 17.8 %copy-start.29 = (pred[8]{0:T(512)(128)(4,1)S(1)}, pred[8]{0:T(512)(128)(4,1)}, u32[]{:S(2)}) copy-start(pred[8]{0:T(512)(128)(4,1)} %copy-done.28) | copy-start | bytes 28
  130.7 17.8 %copy-start.31 = (pred[8]{0:T(512)(128)(4,1)S(1)}, pred[8]{0:T(512)(128)(4,1)}, u32[]{:S(2)}) copy-start(pred[8]{0:T(512)(128)(4,1)} %copy-done.30) | copy-start | bytes 28
  153.2 38.4 %copy-start.10 = (f32[256,256]{0,1:T(8,128)S(1)}, f32[256,256]{0,1:T(8,128)}, u32[]{:S(2)}) copy-start(f32[256,256]{0,1:T(8,128)} %convert_element_type.101) | copy-start | bytes 786436
  194.3 2.1 copy-start.17
  197.6 9.3 %copy-start.13 = (f32[4,2,64,64]{3,2,1,0:T(8,128)S(1)}, f32[4,2,64,64]{3,2,1,0:T(8,128)}, u32[]{:S(2)}) copy-start(f32[4,2,64,64]{3,2,1,0:T(8,128)} %convolution_select_fusion) | copy-start | bytes 393220
  206.9 1.6 copy-start.24
  208.3 3.4 copy-start.7
  209.8 36.8 %copy-start.1 = (f32[4,64,2,128]{1,0,3,2:T(4,128)S(1)}, f32[4,64,2,128]{1,0,3,2:T(4,128)}, u32[]{:S(2)}) copy-start(f32[4,64,2,128]{1,0,3,2:T(4,128)} %reshape.255) | copy-start | bytes 786436
  210.5 36.3 %copy-start.2 = (f32[4,64,2,128]{1,0,3,2:T(4,128)S(1)}, f32[4,64,2,128]{1,0,3,2:T(4,128)}, u32[]{:S(2)}) copy-start(f32[4,64,2,128]{1,0,3,2:T(4,128)} %reshape.256) | copy-start | bytes 786436
  246.8 2.0 copy-start.22
  251.0 2.9 copy-start.15
  253.9 1.6 copy-start.21
  253.9 1.8 copy-start.26
  253.9 1.8 copy-start.32
  256.0 1.2 copy-start.14
  258.7 93.3 %all-gather.8.cloned.1.call-start = ((), (), s32[]{:S(2)}) async-start(), calls=%async_computation.2 | async-start | bytes 6488064 | tf_op jit(solution)/shard_map/all_gather | solution.py:237
  259.3 185.1 %all-gather.10.cloned.1.call-start = ((), (), s32[]{:S(2)}) async-start(), calls=%async_computation.3 | async-start | bytes 6488064 | tf_op jit(solution)/shard_map/all_gather | solution.py:238
  259.8 277.5 %all-gather.12.cloned.1.call-start = ((), (), s32[]{:S(2)}) async-start(), calls=%async_computation.4 | async-start | bytes 6488064 | tf_op jit(solution)/shard_map/all_gather | solution.py:243
  260.4 91.6 %copy-start.33 = (f32[2048]{0:T(1024)S(1)}, f32[2048]{0:T(1024)}, u32[]{:S(2)}) copy-start(f32[2048]{0:T(1024)} %param.42) | copy-start | bytes 24580
  260.4 309.9 %reduce-scatter.2.cloned.1.call-start = ((), (), s32[]{:S(2)}) async-start(), calls=%async_computation.5 | async-start | bytes 1310720 | tf_op jit(solution)/shard_map/reduce_scatter | solution.py:244
Sparse Core Ops, SparseCore 0:
  258.8 35.0 all-reduce.1
  547.4 22.9 reduce-scatter.1
Sparse Core Ops, SparseCore 1:
  261.3 90.6 all-gather.7
  354.1 90.2 all-gather.9
  446.3 91.0 all-gather.11
where the time goes:
time: 581 us; the launch traced here: 580 us
  waiting for transfers between devices  293 us (50%)
  blocking collectives  171 us (29%)
  matrix products  50.9 us (9%)
  local copies, waits for them, and re-layouts  33.3 us (6%)
  between operations  16.2 us (3%)
  other arithmetic  14.3 us (2%)
    all_gather x1, waiting for transfers between devices, per_device(): down_whole = lax.all_gather(down_weight, 'sp', axis=1, tiled=True)  93 us
    all_gather x1, waiting for transfers between devices, per_device(): lax.all_gather(up_weight, 'sp', axis=0, tiled=True)  86.1 us
    all_gather x1, waiting for transfers between devices, per_device(): lax.all_gather(gate_weight, 'sp', axis=0, tiled=True)  56.1 us
    all_gather x1, blocking collectives, per_device(): lax.all_gather(behind_second[1][None].astype(jnp.bfloat16), 'sp', axis=0,...  33.5 us
    psum x1, waiting for transfers between devices, per_device(): lax.psum((jnp.dot(first_group_output, first_output_weight, preferred_elem...  33.2 us
    all_gather x1, blocking collectives, per_device(): lax.all_gather(ahead_second[1][None].astype(jnp.bfloat16), 'sp', axis=0,...  33.2 us
    all_gather x1, blocking collectives, per_device(): lax.all_gather(ahead_first[1][None].astype(jnp.bfloat16), 'sp', axis=0, t...  32.8 us
    all_gather x1, blocking collectives, per_device(): lax.all_gather(behind_first[1][None].astype(jnp.bfloat16), 'sp', axis=0,...  32.8 us
  transfers between devices with their start and end apart: 5, of which 5 were waited for; matrix products, arithmetic and copies ran while one was open for 1% of the time, Pallas kernels for 0%

commit v1 on v0

--- a/solution.py
+++ b/solution.py
@@ -168,9 +168,15 @@
         lax.all_gather(ahead_first[1][None].astype(jnp.bfloat16), "sp", axis=0, tiled=True).astype(
             jnp.float32
         ),
-        lax.all_gather(behind_first[1][None].astype(jnp.bfloat16), "sp", axis=0, tiled=True).astype(
-            jnp.float32
-        ),
+        jnp.concatenate(
+            lax.all_to_all(
+                jnp.stack([behind_first[1][None].astype(jnp.bfloat16)] * lax.axis_size("sp")),
+                "sp",
+                0,
+                0,
+            ),
+            axis=0,
+        ).astype(jnp.float32),
         lax.all_gather(ahead_second[1][None].astype(jnp.bfloat16), "sp", axis=0, tiled=True).astype(
             jnp.float32
         ),

time: 581 us -> 598 us (1.029)
  blocking collectives: 171 us -> 135 us
  matrix products: 50.9 us -> 73.7 us
  local copies, waits for them, and re-layouts: 33.3 us -> 53 us
  starting transfers between devices: 0.39 us -> 7.73 us
    all_gather x1 -> x0, blocking collectives: 32.8 us -> none  [per_device(): lax.all_gather(behind_first[1][None].astype(jnp.bfloat16), 'sp', axis=0,...]
    dot_general x16, matrix products: 9.05 us -> 19.1 us  [advance(): jnp.einsum('hjd,hjv->hdv', key_part, value_part, precision=highest)]
    dot_general x16, matrix products: 8.46 us -> 17.7 us  [advance(): emitted = jnp.einsum('hid,hdv->hiv', query_part, states, precision=highest)]
    all_to_all x0 -> x1, starting transfers between devices: none -> 7.31 us  [per_device(): lax.all_to_all(jnp.stack([behind_first[1][None].astype(jnp.bfloat16)] * l...]
    all_gather x1, waiting for transfers between devices: 86.1 us -> 92.4 us  [per_device(): lax.all_gather(up_weight, 'sp', axis=0, tiled=True)]
    all_gather x1, waiting for transfers between devices: 93 us -> 86.7 us  [per_device(): down_whole = lax.all_gather(down_weight, 'sp', axis=1, tiled=True)]
  transfers between devices with their start and end apart: 5 -> 6, of which waited for: 5 -> 5; matrix products, arithmetic and copies ran while one was open for 1% -> 18% of each run, Pallas kernels for 0% -> 0%
where the time goes in v1:
time: 598 us; the launch traced here: 595 us
  waiting for transfers between devices  293 us (49%)
  blocking collectives  135 us (23%)
  matrix products  73.7 us (12%)
  local copies, waits for them, and re-layouts  53 us (9%)
  other arithmetic  16.3 us (3%)
  between operations  16 us (3%)
  starting transfers between devices  7.73 us (1%)
    all_gather x1, waiting for transfers between devices, per_device(): lax.all_gather(up_weight, 'sp', axis=0, tiled=True)  92.4 us
    all_gather x1, waiting for transfers between devices, per_device(): down_whole = lax.all_gather(down_weight, 'sp', axis=1, tiled=True)  86.7 us
    all_gather x1, waiting for transfers between devices, per_device(): lax.all_gather(gate_weight, 'sp', axis=0, tiled=True)  56.1 us
    all_gather x1, blocking collectives, per_device(): lax.all_gather(behind_second[1][None].astype(jnp.bfloat16), 'sp', axis=0,...  33.4 us
    psum x1, waiting for transfers between devices, per_device(): lax.psum((jnp.dot(first_group_output, first_output_weight, preferred_elem...  33.3 us
    all_gather x1, blocking collectives, per_device(): lax.all_gather(ahead_second[1][None].astype(jnp.bfloat16), 'sp', axis=0,...  33.2 us
    all_gather x1, blocking collectives, per_device(): lax.all_gather(ahead_first[1][None].astype(jnp.bfloat16), 'sp', axis=0, t...  30.8 us
    reduce_scatter x1, waiting for transfers between devices, per_device(): lax.psum_scatter(jnp.dot(hidden, down_whole, preferred_element_type=jnp.f...  23.1 us
  transfers between devices with their start and end apart: 6, of which 5 were waited for; matrix products, arithmetic and copies ran while one was open for 18% of the time, Pallas kernels for 0%

profile of v1, /device:TPU:0, one launch (start us, length us, event | category | flops | bytes accessed | tf_op | source)
XLA Modules:
  0.0 594.9 jit_solution(10206107375939344454)
XLA Ops:
  14.0 7.3 %all-to-all-start = ((bf16[8,1,2,64,128]{4,3,2,1,0:T(8,128)(2,1)}), bf16[8,1,2,64,128]{4,3,2,1,0:T(8,128)(2,1)}, u32[]{:S(2)}, u32[]{:S(2)}) async-start(bf16[8,1,2,64,128]{4,3,2,1,0:T(8,128)(2,1)} %stack.2), calls=%async_computation | async-start | bytes 524288 | tf_op jit(solution)/shard_map/all_to_all | solution.py:172
  31.6 20.9 %all_gather.24 = f32[8,2,64]{2,1,0:T(2,128)S(1)} all-gather(f32[1,2,64]{2,1,0:T(2,128)S(1)} %broadcast_in_dim.108), channel_id=1, replica_groups=mesh['sp'=8,'tp'=4] {'sp'}, dimensions={0}, use_global_device_ids=true | all-gather | bytes 4608 | tf_op jit(solution)/shard_map/all_gather | solution.py:144
  60.2 30.8 %all-gather = bf16[16,64,128]{2,1,0:T(8,128)(2,1)S(1)} all-gather(bf16[2,64,128]{2,1,0:T(8,128)(2,1)S(1)} %convolution_convert_fusion.3), channel_id=2, replica_groups=mesh['sp'=8,'tp'=4] {'sp'}, dimensions={0}, use_global_device_ids=true | all-gather | bytes 294912 | tf_op jit(solution)/shard_map/all_gather | solution.py:168
  92.6 1.8 reshape_reshape.32
  94.4 1.5 fusion.73
  97.5 11.3 %while.48 = (s32[]{:T(128)}, f32[2,64,128]{2,1,0:T(8,128)S(1)}, f32[4,2,64,128]{3,2,1,0:T(8,128)}, f32[4,2,1,64]{3,1,2,0:T(2,128)S(1)}, f32[4,2,64,64]{3,2,1,0:T...) while((s32[]{:T(128)}, f32[2,64,128]{2,1,0:T(8,128)S(1)}, ...), condition=%wide.region_6.7_spmd, body=%wide.region_5.6_spmd.sunk | while | flops 25198592 | bytes 592989 | solution.py:54
  109.4 1.3 fusion.45
  112.7 16.5 %all_gather.26 = f32[8,2,128]{2,1,0:T(2,128)S(1)} all-gather(f32[1,2,128]{2,1,0:T(2,128)S(1)} %bitcast.423), channel_id=1, replica_groups=mesh['sp'=8,'tp'=4] {'sp'}, dimensions={0}, use_global_device_ids=true | all-gather | bytes 9216 | tf_op jit(solution)/shard_map/all_gather | solution.py:145
  134.5 1.9 rev.40
  137.5 1.4 convolution_convert_fusion.1
  138.9 33.4 %all-gather.2 = bf16[16,128,128]{2,1,0:T(8,128)(2,1)} all-gather(bf16[2,128,128]{2,1,0:T(8,128)(2,1)S(1)} %convolution_convert_fusion.1), channel_id=4, replica_groups=mesh['sp'=8,'tp'=4] {'sp'}, dimensions={0}, use_global_device_ids=true | all-gather | bytes 589824 | tf_op jit(solution)/shard_map/all_gather | solution.py:183
  173.5 3.1 rev.37
  177.7 1.3 convolution_select_fusion
  179.9 2.1 fusion.46
  182.7 11.9 %while.51 = (s32[]{:T(128)}, f32[2,128,128]{2,1,0:T(8,128)S(1)}, f32[4,2,64,128]{3,2,1,0:T(8,128)}, f32[4,2,1,128]{3,1,2,0:T(2,128)S(1)}, f32[4,2,64,128]{3,2,1,...) while((s32[]{:T(128)}, f32[2,128,128]{2,1,0:T(8,128)S(1)}, ...), condition=%wide.region_26.27_spmd, body=%wide.region_25.26_spmd.sunk | while | flops 50397184 | bytes 660569 | solution.py:54
  182.7 1.7 fusion.185
  184.4 1.2 convolution_add_fusion.16
  185.7 1.7 fusion.185
  187.4 1.2 convolution_add_fusion.16
  188.7 1.7 fusion.185
  190.4 1.2 convolution_add_fusion.16
  191.7 1.7 fusion.185
  193.4 1.2 convolution_add_fusion.16
  194.6 1.3 fusion.42
  196.2 1.5 copy.329
  202.0 33.2 %all-gather.1 = bf16[16,128,128]{2,1,0:T(8,128)(2,1)} all-gather(bf16[2,128,128]{2,1,0:T(8,128)(2,1)S(1)} %convolution_convert_fusion.2), channel_id=3, replica_groups=mesh['sp'=8,'tp'=4] {'sp'}, dimensions={0}, use_global_device_ids=true | all-gather | bytes 589824 | tf_op jit(solution)/shard_map/all_gather | solution.py:180
  235.6 1.2 copy.284
  236.9 1.2 copy.290
  238.1 1.3 convolution_select_fusion.1
  241.3 2.3 fusion.48
  243.6 9.6 %while.50 = (s32[]{:T(128)}, f32[2,128,128]{2,1,0:T(8,128)S(1)}, f32[4,2,64,128]{3,2,1,0:T(8,128)S(1)}, f32[4,2,1,128]{3,1,2,0:T(2,128)S(1)}, f32[4,2,64,128]{3,...) while((s32[]{:T(128)}, f32[2,128,128]{2,1,0:T(8,128)S(1)}, ...), condition=%wide.region_20.21_spmd, body=%wide.region_19.20_spmd.sunk | while | flops 50397184 | bytes 791133 | solution.py:54
  244.8 1.3 convolution_add_fusion.15
  247.2 1.3 convolution_add_fusion.15
  249.6 1.3 convolution_add_fusion.15
  252.0 1.3 convolution_add_fusion.15
  258.9 1.6 fusion.71
  261.3 7.9 %while.49 = (s32[]{:T(128)}, f32[2,64,128]{2,1,0:T(8,128)S(1)}, f32[4,2,64,128]{3,2,1,0:T(8,128)}, f32[4,2,1,64]{3,1,2,0:T(2,128)S(1)}, f32[4,2,64,64]{3,2,1,0:T...) while((s32[]{:T(128)}, f32[2,64,128]{2,1,0:T(8,128)S(1)}, ...), condition=%wide.region_12.13_spmd, body=%wide.region_11.12_spmd.sunk | while | flops 25198592 | bytes 462937 | solution.py:54
  269.3 1.3 fusion.44
  272.4 1.5 fusion.41
  276.0 33.3 %all-reduce.2.cloned.1.call-done = bf16[256,2048]{1,0:T(8,128)(2,1)} async-done(((bf16[256,2048]{1,0:T(8,128)(2,1)}), bf16[256,2048]{1,0:T(8,128)(2,1)}) %all-reduce.2.cloned.1.call-update) | async-done | bytes 1048592 | tf_op jit(solution)/shard_map/psum | solution.py:232
  309.2 2.0 convert_add_fusion
  311.2 56.1 %all-gather.7.cloned.1.call-done = bf16[2048,1408]{1,0:T(8,128)(2,1)} async-done(((bf16[256,1408]{1,0:T(8,128)(2,1)}), bf16[2048,1408]{1,0:T(8,128)(2,1)}) %all-gather.7.cloned.1.call-update) | async-done | bytes 5767184 | tf_op jit(solution)/shard_map/all_gather | solution.py:243
  367.3 6.3 %fusion.112 = f32[256,1408]{1,0:T(8,128)} fusion(bf16[2048,1408]{1,0:T(8,128)(2,1)} %all-gather.7.cloned.1.call-done, f32[2048]{0:T(1024)S(1)} %copy-done.26, f32[256]{0:T(256)S(1)} %add_rsqrt_fusion.2, bf16[256,2048]{1,0:T(8,128)(2,1)} %all-reduce.2.cloned.1.call-done, bf16[256,2048]{1,0:T(8,128)(2,1)} %param.27), kind=kOutput, calls=%fused_computation.189 | convolution fusion | flops 1479540736 | bytes 9315328 | tf_op jit(solution)/shard_map/dot_general | solution.py:246
  373.6 86.7 %all-gather.11.cloned.1.call-done = bf16[1408,2048]{1,0:T(8,128)(2,1)} async-done(((bf16[1408,256]{1,0:T(8,128)(2,1)}), bf16[1408,2048]{1,0:T(8,128)(2,1)}) %all-gather.11.cloned.1.call-update) | async-done | bytes 5767184 | tf_op jit(solution)/shard_map/all_gather | solution.py:249
  460.3 92.4 %all-gather.9.cloned.1.call-done = bf16[2048,1408]{1,0:T(8,128)(2,1)} async-done(((bf16[256,1408]{1,0:T(8,128)(2,1)}), bf16[2048,1408]{1,0:T(8,128)(2,1)}) %all-gather.9.cloned.1.call-update) | async-done | bytes 5767184 | tf_op jit(solution)/shard_map/all_gather | solution.py:244
  552.7 9.9 %convolution_convert_fusion = bf16[256,2048]{1,0:T(8,128)(2,1)} fusion(bf16[1408,2048]{1,0:T(8,128)(2,1)} %all-gather.11.cloned.1.call-done, bf16[2048,1408]{1,0:T(8,128)(2,1)} %all-gather.9.cloned.1.call-done, f32[256,1408]{1,0:T(8,128)} %fusion.112, f32[2048]{0:T(1024)S(1)} %copy-done.26, f32[256]{0:T(256)S(1)} %add_rsqrt_fusion.2, ...), kind=kOutput, calls=%fused_computation.60 | convolution fusion | flops 2958622720 | bytes 16131072 | tf_op jit(solution)/shard_map/dot_general | solution.py:251
  562.6 23.1 %reduce-scatter.2.cloned.1.call-done = bf16[64,2048]{1,0:T(8,128)(2,1)} async-done(((bf16[256,2048]{1,0:T(8,128)(2,1)}), bf16[64,2048]{1,0:T(8,128)(2,1)}) %reduce-scatter.2.cloned.1.call-update) | async-done | bytes 262160 | tf_op jit(solution)/shard_map/reduce_scatter | solution.py:250
  585.6 1.7 add_convert_fusion
  (248 shorter events, 80.7 us)
Async XLA Ops:
  7.4 264.1 %copy-start = (bf16[256,2048]{1,0:T(8,128)(2,1)S(1)}, bf16[256,2048]{1,0:T(8,128)(2,1)}, u32[]{:S(2)}) copy-start(bf16[256,2048]{1,0:T(8,128)(2,1)} %param.40) | copy-start | bytes 3145732
  7.4 4.8 copy-start.4
  12.2 10.6 %copy-start.17 = (bf16[256,128]{1,0:T(8,128)(2,1)S(1)}, bf16[256,128]{1,0:T(8,128)(2,1)}, u32[]{:S(2)}) copy-start(bf16[256,128]{1,0:T(8,128)(2,1)} %param.28) | copy-start | bytes 196612
  13.2 13.0 %copy-start.15 = (bf16[256,256]{1,0:T(8,128)(2,1)S(1)}, bf16[256,256]{1,0:T(8,128)(2,1)}, u32[]{:S(2)}) copy-start(bf16[256,256]{1,0:T(8,128)(2,1)} %param.33) | copy-start | bytes 393220
  14.0 245.0 %all-to-all-start = ((bf16[8,1,2,64,128]{4,3,2,1,0:T(8,128)(2,1)}), bf16[8,1,2,64,128]{4,3,2,1,0:T(8,128)(2,1)}, u32[]{:S(2)}, u32[]{:S(2)}) async-start(bf16[8,1,2,64,128]{4,3,2,1,0:T(8,128)(2,1)} %stack.2), calls=%async_computation | async-start | bytes 524288 | tf_op jit(solution)/shard_map/all_to_all | solution.py:172
  21.3 287.9 %all-reduce.2.cloned.1.call-start = ((), (), s32[]{:S(2)}) async-start(), calls=%async_computation.2 | async-start | bytes 2097152 | tf_op jit(solution)/shard_map/psum | solution.py:232
  21.5 6.6 %copy-start.16 = (bf16[256,256]{1,0:T(8,128)(2,1)S(1)}, bf16[256,256]{1,0:T(8,128)(2,1)}, u32[]{:S(2)}) copy-start(bf16[256,256]{1,0:T(8,128)(2,1)} %param.34) | copy-start | bytes 393220
  21.8 30.8 %copy-start.21 = (pred[8]{0:T(512)(128)(4,1)}, pred[8]{0:T(512)(128)(4,1)S(1)}, u32[]{:S(2)}) copy-start(pred[8]{0:T(512)(128)(4,1)S(1)} %get-tuple-element.377) | copy-start | bytes 28
  21.8 30.8 %copy-start.23 = (pred[8]{0:T(512)(128)(4,1)}, pred[8]{0:T(512)(128)(4,1)S(1)}, u32[]{:S(2)}) copy-start(pred[8]{0:T(512)(128)(4,1)S(1)} %get-tuple-element.378) | copy-start | bytes 28
  23.0 6.3 %copy-start.5 = (bf16[256,256]{1,0:T(8,128)(2,1)S(1)}, bf16[256,256]{1,0:T(8,128)(2,1)}, u32[]{:S(2)}) copy-start(bf16[256,256]{1,0:T(8,128)(2,1)} %param.35) | copy-start | bytes 393220
  53.8 37.2 %copy-start.9 = (f32[4,64,2,64]{1,0,3,2:T(4,128)S(1)}, f32[4,64,2,64]{1,0,3,2:T(4,128)}, u32[]{:S(2)}) copy-start(f32[4,64,2,64]{1,0,3,2:T(4,128)} %reshape_reshape.29) | copy-start | bytes 393220
  108.7 3.7 copy-start.20
  109.4 19.8 %copy-start.22 = (pred[8]{0:T(512)(128)(4,1)S(1)}, pred[8]{0:T(512)(128)(4,1)}, u32[]{:S(2)}) copy-start(pred[8]{0:T(512)(128)(4,1)} %copy-done.21) | copy-start | bytes 28
  109.4 19.8 %copy-start.24 = (pred[8]{0:T(512)(128)(4,1)S(1)}, pred[8]{0:T(512)(128)(4,1)}, u32[]{:S(2)}) copy-start(pred[8]{0:T(512)(128)(4,1)} %copy-done.23) | copy-start | bytes 28
  112.7 18.8 %copy-start.18 = (f32[256]{0:T(256)}, f32[256]{0:T(256)S(1)}, u32[]{:S(2)}) copy-start(f32[256]{0:T(256)S(1)} %get-tuple-element.364) | copy-start | bytes 3076
  177.7 2.2 copy-start.2
  177.7 2.2 copy-start.14
  182.0 12.7 %copy-start.3 = (f32[256,2,128]{2,0,1:T(8,128)S(1)}, f32[256,2,128]{2,0,1:T(8,128)}, u32[]{:S(2)}) copy-start(f32[256,2,128]{2,0,1:T(8,128)} %copy.308) | copy-start | bytes 786436
  182.0 12.7 %copy-start.10 = (f32[4,2,64,64]{3,2,1,0:T(8,128)S(1)}, f32[4,2,64,64]{3,2,1,0:T(8,128)}, u32[]{:S(2)}) copy-start(f32[4,2,64,64]{3,2,1,0:T(8,128)} %convolution_select_fusion) | copy-start | bytes 393220
  196.0 5.7 copy-start.6
  196.0 5.7 copy-start.19
  196.2 39.0 %copy-start.8 = (f32[256,256]{1,0:T(8,128)S(1)}, f32[256,256]{1,0:T(8,128)}, u32[]{:S(2)}) copy-start(f32[256,256]{1,0:T(8,128)} %copy.286) | copy-start | bytes 786436
  243.6 9.6 %copy-start.7 = (f32[4,2,64,64]{3,2,1,0:T(8,128)S(1)}, f32[4,2,64,64]{3,2,1,0:T(8,128)}, u32[]{:S(2)}) copy-start(f32[4,2,64,64]{3,2,1,0:T(8,128)} %convolution_select_fusion.1) | copy-start | bytes 393220
  261.3 9.5 %copy-start.1 = (f32[4,64,2,128]{3,1,0,2:T(8,128)S(1)}, f32[4,64,2,128]{3,1,0,2:T(8,128)}, u32[]{:S(2)}) copy-start(f32[4,64,2,128]{3,1,0,2:T(8,128)} %copy.263) | copy-start | bytes 786436
  261.3 9.6 %copy-start.11 = (f32[256,2,128]{2,0,1:T(8,128)S(1)}, f32[256,2,128]{2,0,1:T(8,128)}, u32[]{:S(2)}) copy-start(f32[256,2,128]{2,0,1:T(8,128)} %copy.280) | copy-start | bytes 786436
  261.3 9.7 %copy-start.12 = (f32[256,2,128]{2,0,1:T(8,128)S(1)}, f32[256,2,128]{2,0,1:T(8,128)}, u32[]{:S(2)}) copy-start(f32[256,2,128]{2,0,1:T(8,128)} %copy.320) | copy-start | bytes 786436
  261.3 9.7 %copy-start.25 = (f32[128]{0:T(128)S(1)}, f32[128]{0:T(128)}, u32[]{:S(2)}) copy-start(f32[128]{0:T(128)} %param.39) | copy-start | bytes 1540
  271.2 1.2 copy-start.13
  273.9 93.4 %all-gather.7.cloned.1.call-start = ((), (), s32[]{:S(2)}) async-start(), calls=%async_computation.3 | async-start | bytes 6488064 | tf_op jit(solution)/shard_map/all_gather | solution.py:243
  274.5 185.8 %all-gather.11.cloned.1.call-start = ((), (), s32[]{:S(2)}) async-start(), calls=%async_computation.5 | async-start | bytes 6488064 | tf_op jit(solution)/shard_map/all_gather | solution.py:249
  275.1 277.6 %all-gather.9.cloned.1.call-start = ((), (), s32[]{:S(2)}) async-start(), calls=%async_computation.4 | async-start | bytes 6488064 | tf_op jit(solution)/shard_map/all_gather | solution.py:244
  275.7 91.6 %copy-start.26 = (f32[2048]{0:T(1024)S(1)}, f32[2048]{0:T(1024)}, u32[]{:S(2)}) copy-start(f32[2048]{0:T(1024)} %param.42) | copy-start | bytes 24580
  275.7 310.0 %reduce-scatter.2.cloned.1.call-start = ((), (), s32[]{:S(2)}) async-start(), calls=%async_computation.6 | async-start | bytes 1310720 | tf_op jit(solution)/shard_map/reduce_scatter | solution.py:250
Sparse Core Ops, SparseCore 0:
  274.0 35.1 all-reduce.1
  562.7 22.9 reduce-scatter.1
Sparse Core Ops, SparseCore 1:
  276.6 90.7 all-gather.6
  369.2 91.0 all-gather.10
  462.3 90.3 all-gather.8
